TPU v7x, 32 devices: a whole 2x2x4 slice. The times are simulated.
32 devices in a mesh: sp: 16 (over z, y, x), tp: 2 (over core).
Axes of the slice: x: 2, y: 2, z: 4, core: 2. Of those that a mesh axis runs over, the one named last changes fastest.
Arguments:
- acceptor_signal: bfloat16 [2048, 1024], P('sp', 'tp'), may hold values from -6 to 6
- address_entries: bfloat16 [2048, 1024], P('sp', 'tp'), may hold values from -6 to 6
- payload_entries: bfloat16 [2048, 1024], P('sp', 'tp'), may hold values from -6 to 6
- fading_logits: float32 [2048, 1024], P('sp', 'tp'), may hold values from -12 to -2
- learning_rate_logits: float32 [2048, 1024], P('sp', 'tp'), may hold values from -10 to 4
- exit_switch_entries: bfloat16 [2048, 1024], P('sp', 'tp'), may hold values from -6 to 6
- extra_reward_weights: float32 [1024], P('tp'), may hold values from -0.3 to 0.3
- subspace_rescale_weights: float32 [1024], P('tp'), may hold values from 0.1 to 1.9
- timemix_exit_weights: bfloat16 [1024, 2048], P('tp'), may hold values from -0.1875 to 0.1875
- skip_stream_arriving: bfloat16 [2048, 2048], P(('sp', 'tp')), may hold values from -6 to 6
- pointwise_block_scaling: float32 [2048], replicated, may hold values from 0.1 to 1.9
- switch_projection: bfloat16 [2048, 5632], P('sp', 'tp'), may hold values from -0.125 to 0.125
- widening_projection: bfloat16 [2048, 5632], P('sp', 'tp'), may hold values from -0.125 to 0.125
- switch_filter_coefficients: float32 [3, 5632], P(None, 'tp'), may hold values from -3.5 to 3.5
- narrowing_projection: bfloat16 [5632, 2048], P('tp', 'sp'), may hold values from -0.078125 to 0.078125
Outputs:
- layer_out: bfloat16 [2048, 2048], P(('sp', 'tp'))
All inputs are finite; a program needn't handle non-finite values.
Results may differ from a plain program's by a relative error of at most 0.019.
Values may be sent and summed in bfloat16 or wider, within the bound.
A program may use at most 128 MiB of HBM per device.

v0:
```python
import jax
import jax.numpy as jnp
from jax import lax
from jax.sharding import PartitionSpec as P

SUBSPACE_WIDTH = 64
SPAN = 16
group_eps = 0.00064
norm_eps = 1e-06
highest = lax.Precision.HIGHEST


def carried_in(shard, axis, join, neutral):
    place = lax.axis_index(axis)
    gathered = jax.tree.map(
        lambda a, kind: lax.all_gather(a.astype(kind), axis), shard, (jnp.bfloat16, jnp.bfloat16)
    )
    state = jax.tree.map(lambda a, e: jnp.zeros_like(a) + jnp.asarray(e, a.dtype), shard, neutral)

    def one(lap, state):
        return join(
            state,
            jax.tree.map(
                lambda a, own: lax.dynamic_index_in_dim(a, lap, 0, False).astype(own.dtype),
                gathered,
                shard,
            ),
        )

    return lax.fori_loop(0, place, one, state)


def shifted(block, axis, distance):
    devices = range(lax.axis_size(axis))
    route = [(i - distance, i) for i in devices if i - distance in devices]
    return lax.ppermute(block, axis, route)


def by_heads(array):
    return array.astype(jnp.float32).reshape(array.shape[0], -1, SUBSPACE_WIDTH)


def mechanism_inputs(
    acceptor_signal, address_entries, payload_entries, fading_logits, learning_rate_logits
):
    acceptor_entries = by_heads(acceptor_signal)
    address_mapped = by_heads(address_entries)
    payload_mapped = by_heads(payload_entries)
    log_rate = -jax.nn.softplus(-fading_logits) - 0.5
    fading = by_heads(jnp.exp(-jnp.exp(log_rate)))
    erase_rate = by_heads(jax.nn.sigmoid(learning_rate_logits))
    length = jnp.sqrt(jnp.sum(address_mapped * address_mapped, axis=-1, keepdims=True))
    unit_key = address_mapped / jnp.maximum(length, 1.0)
    return (
        acceptor_entries,
        address_mapped,
        payload_mapped,
        fading,
        -unit_key,
        unit_key * erase_rate,
    )


def subspace_outcomes(
    acceptor_entries,
    address_mapped,
    payload_mapped,
    closing_memory,
    subspace_rescale_weights,
    extra_reward_weights,
    exit_switch_entries,
):
    centred = closing_memory - jnp.mean(closing_memory, axis=-1, keepdims=True)
    rescaled_arguments = centred * lax.rsqrt(
        jnp.mean(centred * centred, axis=-1, keepdims=True) + group_eps
    )
    scaling_fetch = subspace_rescale_weights.reshape(-1, SUBSPACE_WIDTH)
    extra_reward_fetch = extra_reward_weights.reshape(-1, SUBSPACE_WIDTH)
    present_extra_reward = (
        jnp.sum(acceptor_entries * address_mapped * extra_reward_fetch, axis=-1, keepdims=True)
        * payload_mapped
    )
    timemix_product = rescaled_arguments * scaling_fetch + present_extra_reward
    timemix_product = timemix_product.reshape(
        timemix_product.shape[0], -1
    ) * exit_switch_entries.astype(jnp.float32)
    return timemix_product.astype(jnp.bfloat16)


def compose(earlier, latter):
    mapping = jnp.einsum("...ij,...jk->...ik", earlier[0], latter[0], precision=highest)
    state = jnp.einsum("...ij,...jk->...ik", earlier[1], latter[0], precision=highest) + latter[1]
    return (mapping, state)


def span_step(carried, sublevel_arguments):
    state, mapping = carried
    acceptor_entries, address_mapped, payload_mapped, fading, erase_dir, erase_amt = (
        sublevel_arguments
    )
    along = jnp.einsum("bhij,bhj->bhi", state, erase_dir, precision=highest)
    map_along = jnp.einsum("bhij,bhj->bhi", mapping, erase_dir, precision=highest)
    state = (
        state * fading[:, :, None, :]
        + along[..., None] * erase_amt[:, :, None, :]
        + payload_mapped[..., None] * address_mapped[:, :, None, :]
    )
    mapping = mapping * fading[:, :, None, :] + map_along[..., None] * erase_amt[:, :, None, :]
    local_out = jnp.einsum("bhij,bhj->bhi", state, acceptor_entries, precision=highest)
    probe = jnp.einsum("bhij,bhj->bhi", mapping, acceptor_entries, precision=highest)
    return ((state, mapping), (local_out, probe))


def recurrence(sublevel_arguments):
    token_count, head_count = (sublevel_arguments[0].shape[0], sublevel_arguments[0].shape[1])
    blocks = token_count // SPAN

    def arrange(member):
        return jnp.moveaxis(member.reshape(blocks, SPAN, head_count, SUBSPACE_WIDTH), 1, 0)

    arranged = tuple((arrange(member) for member in sublevel_arguments))
    unit_map = jnp.eye(SUBSPACE_WIDTH, dtype=jnp.float32)
    zero_state = jnp.zeros((blocks, head_count, SUBSPACE_WIDTH, SUBSPACE_WIDTH), jnp.float32)
    start_maps = jnp.broadcast_to(unit_map, zero_state.shape)
    (block_states, block_maps), (local_out, probe) = lax.scan(
        span_step, (zero_state, start_maps), arranged
    )
    cum_maps, cum_states = lax.associative_scan(compose, (block_maps, block_states))
    head_unit = jnp.broadcast_to(unit_map, (head_count, SUBSPACE_WIDTH, SUBSPACE_WIDTH))
    head_zero = jnp.zeros((head_count, SUBSPACE_WIDTH, SUBSPACE_WIDTH), jnp.float32)
    _, incoming = carried_in((cum_maps[-1], cum_states[-1]), "sp", compose, (head_unit, head_zero))
    prior_maps = jnp.concatenate([head_unit[None], cum_maps[:-1]], axis=0)
    prior_states = jnp.concatenate([head_zero[None], cum_states[:-1]], axis=0)
    entry = jnp.einsum("hij,bhjk->bhik", incoming, prior_maps, precision=highest) + prior_states
    closing_memory = local_out + jnp.einsum("bhij,tbhj->tbhi", entry, probe, precision=highest)
    return jnp.moveaxis(closing_memory, 0, 1).reshape(token_count, head_count, SUBSPACE_WIDTH)


def body(
    acceptor_signal,
    address_entries,
    payload_entries,
    fading_logits,
    learning_rate_logits,
    exit_switch_entries,
    extra_reward_weights,
    subspace_rescale_weights,
    timemix_exit_weights,
    skip_stream_arriving,
    pointwise_block_scaling,
    switch_projection,
    widening_projection,
    switch_filter_coefficients,
    narrowing_projection,
):
    gate_full, up_full, down_full = (
        lax.all_gather(switch_projection, "sp", axis=0, tiled=True),
        lax.all_gather(widening_projection, "sp", axis=0, tiled=True),
        lax.all_gather(narrowing_projection, "sp", axis=1, tiled=True),
    )
    sublevel_arguments = mechanism_inputs(
        acceptor_signal, address_entries, payload_entries, fading_logits, learning_rate_logits
    )
    closing_memory = recurrence(sublevel_arguments)
    timemix_product = subspace_outcomes(
        sublevel_arguments[0],
        sublevel_arguments[1],
        sublevel_arguments[2],
        closing_memory,
        subspace_rescale_weights,
        extra_reward_weights,
        exit_switch_entries,
    )
    token_count = timemix_product.shape[0]
    picked = timemix_product
    attended = lax.psum_scatter(
        jnp.dot(picked, timemix_exit_weights, preferred_element_type=jnp.float32).astype(
            jnp.bfloat16
        ),
        "tp",
        scatter_dimension=0,
        tiled=True,
    ).astype(jnp.float32)
    hidden_res = skip_stream_arriving.astype(jnp.float32) + attended
    rescaled_arguments = (
        hidden_res
        * lax.rsqrt(jnp.mean(hidden_res * hidden_res, axis=-1, keepdims=True) + norm_eps)
        * pointwise_block_scaling
    )
    rescaled_arguments = rescaled_arguments.astype(jnp.bfloat16)
    all_rows = lax.all_gather(rescaled_arguments, "tp", axis=0, tiled=True)
    gate_acc = jnp.dot(all_rows, gate_full, preferred_element_type=jnp.float32)
    up_acc = jnp.dot(all_rows, up_full, preferred_element_type=jnp.float32)
    gate_pre = gate_acc.astype(jnp.bfloat16)
    up_part = up_acc.astype(jnp.bfloat16)
    taps = switch_filter_coefficients.shape[0]
    tail_rows = shifted(gate_pre[token_count - taps + 1 :], "sp", 1)
    extended = jnp.concatenate([tail_rows, gate_pre], axis=0).astype(jnp.float32)
    conv_out = jnp.zeros(gate_pre.shape, jnp.float32)
    for tap in range(taps):
        conv_out = conv_out + switch_filter_coefficients[tap] * extended[tap : tap + token_count]
    hidden = (jax.nn.silu(conv_out) * up_part.astype(jnp.float32)).astype(jnp.bfloat16)
    picked = hidden
    projected = lax.psum_scatter(
        jnp.dot(picked, down_full, preferred_element_type=jnp.float32).astype(jnp.bfloat16),
        "tp",
        scatter_dimension=0,
        tiled=True,
    ).astype(jnp.float32)
    return (hidden_res + projected).astype(jnp.bfloat16)


def solution(mesh):
    return jax.shard_map(
        body,
        mesh=mesh,
        in_specs=(
            P("sp", "tp"),
            P("sp", "tp"),
            P("sp", "tp"),
            P("sp", "tp"),
            P("sp", "tp"),
            P("sp", "tp"),
            P("tp"),
            P("tp"),
            P("tp", None),
            P(("sp", "tp"), None),
            P(),
            P("sp", "tp"),
            P("sp", "tp"),
            P(None, "tp"),
            P("tp", "sp"),
        ),
        out_specs=P(("sp", "tp"), None),
        check_vma=False,
    )
```

profile of v0, /device:TPU:0, one launch (start us, length us, event | category | flops | bytes accessed | tf_op | source)
XLA Modules:
  0.0 1192.7 jit_solution(1004884859613980477)
XLA Ops:
  23.3 418.0 %while.30 = (s32[]{:T(128)}, f32[8,8,64,64]{3,2,1,0:T(8,128)}, f32[8,8,64,64]{3,2,1,0:T(8,128)}, f32[16,8,8,64]{3,0,2,1:T(8,128)}, f32[16,8,8,64]{3,0,2,1:T(8,12...) while((s32[]{:T(128)}, f32[8,8,64,64]{3,2,1,0:T(8,128)}, ...), condition=%wide.region_2.3_spmd.clone, body=%wide.region_1.2_spmd.clone.sunk | while | flops 15204355 | bytes 25657612 | solution.py:125
  48.5 5.1 fusion.113
  74.8 5.1 fusion.113
  101.0 5.1 fusion.113
  127.2 5.1 fusion.113
  153.4 5.1 fusion.113
  452.4 9.2 pad.48
  463.5 9.2 pad.47
  478.5 16.6 %pad.50 = f32[8,8,64,64]{3,2,1,0:T(8,128)} pad(f32[4,8,64,64]{3,2,1,0:T(8,128)} %copy-done.6, f32[]{:T(128)} %constant.54.clone.1), padding=1_0_1x0_0_0x0_0_0x0_0_0 | pad | bytes 1572868 | tf_op jit(solution)/shard_map/pad | solution.py:128
  497.4 16.7 %pad.49 = f32[8,8,64,64]{3,2,1,0:T(8,128)} pad(f32[4,8,64,64]{3,2,1,0:T(8,128)} %pad_maximum_fusion.1, f32[]{:T(128)} %constant.54.clone.1), padding=0_1_1x0_0_0x0_0_0x0_0_0 | pad | bytes 1572868 | tf_op jit(solution)/shard_map/pad | solution.py:128
  518.8 5.9 pad.41
  525.8 5.9 pad.42
  533.4 11.1 pad.112
  546.2 16.6 %pad.67 = f32[7,8,64,64]{3,2,1,0:T(8,128)} pad(f32[4,8,64,64]{3,2,1,0:T(8,128)} %pad_maximum_fusion.1, f32[]{:T(128)} %constant.54.clone.1), padding=0_0_1x0_0_0x0_0_0x0_0_0 | pad | bytes 1441796 | tf_op jit(solution)/shard_map/slice | solution.py:133
  563.8 11.2 pad.44
  577.1 11.2 pad.43
  594.9 46.1 %all-gather.6.cloned.1.call-done = bf16[16,8,64,64]{3,2,1,0:T(8,128)(2,1)} async-done(((bf16[1,8,64,64]{3,2,1,0:T(8,128)(2,1)}), bf16[16,8,64,64]{3,2,1,0:T(8,128)(2,1)}) %all-gather.6.cloned.1.call-update) | async-done | bytes 1048592 | tf_op jit(solution)/shard_map/all_gather | solution.py:16
  654.4 39.6 %reduce-scatter.3.cloned.1.call-done = bf16[64,2048]{1,0:T(8,128)(2,1)} async-done(((bf16[128,2048]{1,0:T(8,128)(2,1)}), bf16[64,2048]{1,0:T(8,128)(2,1)}) %reduce-scatter.3.cloned.1.call-update) | async-done | bytes 262160 | tf_op jit(solution)/shard_map/reduce_scatter | solution.py:176
  698.4 140.8 %all-gather.10.cloned.1.call-done = bf16[2048,2816]{1,0:T(8,128)(2,1)} async-done(((bf16[128,2816]{1,0:T(8,128)(2,1)}), bf16[2048,2816]{1,0:T(8,128)(2,1)}) %all-gather.10.cloned.1.call-update) | async-done | bytes 11534352 | tf_op jit(solution)/shard_map/all_gather | solution.py:157
  839.1 6.0 convolution_convert_fusion.1
  851.0 130.4 %all-gather.12.cloned.1.call-done = bf16[2048,2816]{1,0:T(8,128)(2,1)} async-done(((bf16[128,2816]{1,0:T(8,128)(2,1)}), bf16[2048,2816]{1,0:T(8,128)(2,1)}) %all-gather.12.cloned.1.call-update) | async-done | bytes 11534352 | tf_op jit(solution)/shard_map/all_gather | solution.py:158
  981.4 182.8 %all-gather.14.cloned.1.call-done = bf16[2816,2048]{1,0:T(8,128)(2,1)} async-done(((bf16[2816,128]{1,0:T(8,128)(2,1)}), bf16[2816,2048]{1,0:T(8,128)(2,1)}) %all-gather.14.cloned.1.call-update) | async-done | bytes 11534352 | tf_op jit(solution)/shard_map/all_gather | solution.py:159
  1164.2 13.6 %convolution_convert_fusion.2 = bf16[128,2048]{1,0:T(8,128)(2,1)} fusion(bf16[2816,2048]{1,0:T(8,128)(2,1)} %all-gather.14.cloned.1.call-done, bf16[128,2048]{1,0:T(8,128)(2,1)S(1)} %all_gather.22, bf16[2048,2816]{1,0:T(8,128)(2,1)} %all-gather.12.cloned.1.call-done, f32[130,2816]{1,0:T(8,128)} %maximum_convert_fusion, f32[2816]{0:T(1024)S(1)} %get-tuple-element.188, ...), kind=kOutput, calls=%fused_computation.27 | convolution fusion | flops 2957737984 | bytes 28476416 | tf_op jit(solution)/shard_map/dot_general | solution.py:205
  1177.8 6.3 reduce-scatter.5.cloned.1.call-done
  (426 shorter events, 473.3 us)
Async XLA Ops:
  6.5 643.8 %copy-start = (bf16[512,2048]{1,0:T(8,128)(2,1)S(1)}, bf16[512,2048]{1,0:T(8,128)(2,1)}, u32[]{:S(2)}) copy-start(bf16[512,2048]{1,0:T(8,128)(2,1)} %param.27) | copy-start | bytes 6291460
  6.5 588.4 %all-gather.8.cloned.1.call-start = ((), (), s32[]{:S(2)}) async-start(), calls=%async_computation.3 | async-start | bytes 2228224 | tf_op jit(solution)/shard_map/all_gather | solution.py:16
  7.9 13.7 %copy-start.21 = (f32[64,64]{1,0:T(8,128)}, f32[64,64]{1,0:T(8,128)S(1)}, u32[]{:S(2)}) copy-start(f32[64,64]{1,0:T(8,128)S(1)} %fusion.61) | copy-start | bytes 49156
  48.5 10.0 copy-start.4
  74.8 10.0 copy-start.4
  101.0 10.0 copy-start.4
  127.2 10.0 copy-start.4
  153.4 10.0 copy-start.4
  179.6 10.0 copy-start.4
  450.7 10.9 slice-start
  478.5 16.6 %copy-start.17 = (f32[1,8,64,64]{3,2,1,0:T(8,128)S(1)}, f32[1,8,64,64]{3,2,1,0:T(8,128)}, u32[]{:S(2)}) copy-start(f32[1,8,64,64]{3,2,1,0:T(8,128)} %slice.129) | copy-start | bytes 393220
  515.8 125.2 %all-gather.6.cloned.1.call-start = ((), (), s32[]{:S(2)}) async-start(), calls=%async_computation.2 | async-start | bytes 2228224 | tf_op jit(solution)/shard_map/all_gather | solution.py:16
  546.1 147.8 %reduce-scatter.3.cloned.1.call-start = ((), (), s32[]{:S(2)}) async-start(), calls=%async_computation.4 | async-start | bytes 786432 | tf_op jit(solution)/shard_map/reduce_scatter | solution.py:176
  577.1 11.3 copy-start.26
  577.1 11.3 copy-start.16
  652.6 41.4 %copy-start.12 = (bf16[64,2048]{1,0:T(8,128)(2,1)S(1)}, bf16[64,2048]{1,0:T(8,128)(2,1)}, u32[]{:S(2)}) copy-start(bf16[64,2048]{1,0:T(8,128)(2,1)} %param.28) | copy-start | bytes 786436
  652.6 42.6 %copy-start.24 = (f32[2048]{0:T(1024)S(1)}, f32[2048]{0:T(1024)}, u32[]{:S(2)}) copy-start(f32[2048]{0:T(1024)} %param.29) | copy-start | bytes 24580
  652.6 186.6 %all-gather.10.cloned.1.call-start = ((), (), s32[]{:S(2)}) async-start(), calls=%async_computation.5 | async-start | bytes 12255232 | tf_op jit(solution)/shard_map/all_gather | solution.py:157
  653.2 328.2 %all-gather.12.cloned.1.call-start = ((), (), s32[]{:S(2)}) async-start(), calls=%async_computation.6 | async-start | bytes 12255232 | tf_op jit(solution)/shard_map/all_gather | solution.py:158
  653.7 510.5 %all-gather.14.cloned.1.call-start = ((), (), s32[]{:S(2)}) async-start(), calls=%async_computation.7 | async-start | bytes 12255232 | tf_op jit(solution)/shard_map/all_gather | solution.py:159
  654.3 529.8 %reduce-scatter.5.cloned.1.call-start = ((), (), s32[]{:S(2)}) async-start(), calls=%async_computation.8 | async-start | bytes 786432 | tf_op jit(solution)/shard_map/reduce_scatter | solution.py:204
  698.4 150.2 %copy-start.23 = (f32[3,2816]{1,0:T(4,128)S(1)}, f32[3,2816]{1,0:T(4,128)}, u32[]{:S(2)}) copy-start(f32[3,2816]{1,0:T(4,128)} %param.32) | copy-start | bytes 101380
  845.1 4.6 collective-permute-start
  1164.2 19.9 %copy-start.13 = (bf16[64,2048]{1,0:T(8,128)(2,1)S(1)}, bf16[64,2048]{1,0:T(8,128)(2,1)}, u32[]{:S(2)}) copy-start(bf16[64,2048]{1,0:T(8,128)(2,1)} %reduce-scatter.3.cloned.1.call-done) | copy-start | bytes 786436
  (72 other events, 321.6 us)
Sparse Core Ops, SparseCore 0:
  515.9 63.0 all-gather.7
  581.9 59.1 all-gather.5
  652.7 41.2 reduce-scatter.2
  696.6 142.5 all-gather.9
  841.7 139.5 all-gather.11
  983.9 180.2 all-gather.13
  1178.0 6.0 reduce-scatter.4
where the time goes:
time: 1210 us; the launch traced here: 1190 us
  waiting for transfers between devices  549 us (45%)
  matrix products  311 us (26%)
  local copies, waits for them, and re-layouts  248 us (20%)
  other arithmetic  64.1 us (5%)
  between operations  14.1 us (1%)
    all_gather x1, waiting for transfers between devices, body(): lax.all_gather(narrowing_projection, 'sp', axis=1, tiled=True)  183 us
    all_gather x1, waiting for transfers between devices, body(): lax.all_gather(switch_projection, 'sp', axis=0, tiled=True)  141 us
    all_gather x1, waiting for transfers between devices, body(): lax.all_gather(widening_projection, 'sp', axis=0, tiled=True)  130 us
    pad x8, local copies, waits for them, and re-layouts, recurrence(): lax.associative_scan(compose, (block_maps, block_states))  86 us
    dot_general x16, matrix products, span_step(): along = jnp.einsum('bhij,bhj->bhi', state, erase_dir, precision=highest)  79.9 us
    dot_general x16, matrix products, span_step(): jnp.einsum('bhij,bhj->bhi', state, acceptor_entries, precision=highest)  79 us
    dynamic_update_slice x32, local copies, waits for them, and re-layouts, recurrence(): lax.scan(span_step, (zero_state, start_maps), arranged)  57 us
    dot_general x16, matrix products, span_step(): jnp.einsum('bhij,bhj->bhi', mapping, erase_dir, precision=highest)  53.9 us
  transfers between devices with their start and end apart: 8, of which 7 were waited for; matrix products, arithmetic and copies ran while one was open for 7% of the time, Pallas kernels for 0%

commit v1 on v0

--- a/solution.py
+++ b/solution.py
@@ -156,7 +156,7 @@
     gate_full, up_full, down_full = (
         lax.all_gather(switch_projection, "sp", axis=0, tiled=True),
         lax.all_gather(widening_projection, "sp", axis=0, tiled=True),
-        lax.all_gather(narrowing_projection, "sp", axis=1, tiled=True),
+        jnp.concatenate(lax.all_gather(narrowing_projection, "sp"), axis=1),
     )
     sublevel_arguments = mechanism_inputs(
         acceptor_signal, address_entries, payload_entries, fading_logits, learning_rate_logits

time: 1210 us -> 1170 us (0.967)
  waiting for transfers between devices: 549 us -> 494 us
  local copies, waits for them, and re-layouts: 248 us -> 263 us
    all_gather x1, waiting for transfers between devices: 183 us -> 133 us  [body(): lax.all_gather(narrowing_projection, 'sp')]
    reshape x0 -> x1, local copies, waits for them, and re-layouts: none -> 15.2 us  [body(): jnp.concatenate(lax.all_gather(narrowing_projection, 'sp'), axis=1)]
  transfers between devices with their start and end apart: 8 -> 8, of which waited for: 7 -> 6; matrix products, arithmetic and copies ran while one was open for 7% -> 9% of each run, Pallas kernels for 0% -> 0%
where the time goes in v1:
time: 1170 us; the launch traced here: 1150 us
  waiting for transfers between devices  494 us (42%)
  matrix products  312 us (27%)
  local copies, waits for them, and re-layouts  263 us (22%)
  other arithmetic  64.1 us (5%)
  between operations  14.1 us (1%)
    all_gather x1, waiting for transfers between devices, body(): lax.all_gather(switch_projection, 'sp', axis=0, tiled=True)  141 us
    all_gather x1, waiting for transfers between devices, body(): lax.all_gather(narrowing_projection, 'sp')  133 us
    all_gather x1, waiting for transfers between devices, body(): lax.all_gather(widening_projection, 'sp', axis=0, tiled=True)  126 us
    pad x8, local copies, waits for them, and re-layouts, recurrence(): lax.associative_scan(compose, (block_maps, block_states))  85.3 us
    dot_general x16, matrix products, span_step(): along = jnp.einsum('bhij,bhj->bhi', state, erase_dir, precision=highest)  79.9 us
    dot_general x16, matrix products, span_step(): jnp.einsum('bhij,bhj->bhi', state, acceptor_entries, precision=highest)  79 us
    dynamic_update_slice x32, local copies, waits for them, and re-layouts, recurrence(): lax.scan(span_step, (zero_state, start_maps), arranged)  56.8 us
    dot_general x16, matrix products, span_step(): jnp.einsum('bhij,bhj->bhi', mapping, erase_dir, precision=highest)  53.9 us
  transfers between devices with their start and end apart: 8, of which 6 were waited for; matrix products, arithmetic and copies ran while one was open for 9% of the time, Pallas kernels for 0%

profile of v1, /device:TPU:0, one launch (start us, length us, event | category | flops | bytes accessed | tf_op | source)
XLA Modules:
  0.0 1152.8 jit_solution(1500716186759594818)
XLA Ops:
  23.2 417.7 %while.30 = (s32[]{:T(128)}, f32[8,8,64,64]{3,2,1,0:T(8,128)}, f32[8,8,64,64]{3,2,1,0:T(8,128)}, f32[16,8,8,64]{3,0,2,1:T(8,128)}, f32[16,8,8,64]{3,0,2,1:T(8,12...) while((s32[]{:T(128)}, f32[8,8,64,64]{3,2,1,0:T(8,128)}, ...), condition=%wide.region_2.3_spmd.clone, body=%wide.region_1.2_spmd.clone.sunk | while | flops 15204355 | bytes 25657612 | solution.py:125
  74.7 5.1 fusion.113
  100.9 5.1 fusion.113
  258.2 5.1 fusion.113
  389.3 5.1 fusion.113
  452.2 9.1 pad.48
  463.2 9.2 pad.47
  478.2 16.5 %pad.50 = f32[8,8,64,64]{3,2,1,0:T(8,128)} pad(f32[4,8,64,64]{3,2,1,0:T(8,128)} %copy-done.6, f32[]{:T(128)} %constant.54.clone.1), padding=1_0_1x0_0_0x0_0_0x0_0_0 | pad | bytes 1572868 | tf_op jit(solution)/shard_map/pad | solution.py:128
  497.0 16.6 %pad.49 = f32[8,8,64,64]{3,2,1,0:T(8,128)} pad(f32[4,8,64,64]{3,2,1,0:T(8,128)} %pad_maximum_fusion.1, f32[]{:T(128)} %constant.54.clone.1), padding=0_1_1x0_0_0x0_0_0x0_0_0 | pad | bytes 1572868 | tf_op jit(solution)/shard_map/pad | solution.py:128
  518.3 5.9 pad.41
  525.2 5.8 pad.42
  532.7 11.0 pad.112
  545.4 16.5 %pad.67 = f32[7,8,64,64]{3,2,1,0:T(8,128)} pad(f32[4,8,64,64]{3,2,1,0:T(8,128)} %pad_maximum_fusion.1, f32[]{:T(128)} %constant.54.clone.1), padding=0_0_1x0_0_0x0_0_0x0_0_0 | pad | bytes 1441796 | tf_op jit(solution)/shard_map/slice | solution.py:133
  562.8 11.1 pad.44
  576.0 11.1 pad.43
  593.7 46.9 %all-gather.7.cloned.1.call-done = bf16[16,8,64,64]{3,2,1,0:T(8,128)(2,1)} async-done(((bf16[1,8,64,64]{3,2,1,0:T(8,128)(2,1)}), bf16[16,8,64,64]{3,2,1,0:T(8,128)(2,1)}) %all-gather.7.cloned.1.call-update) | async-done | bytes 1048592 | tf_op jit(solution)/shard_map/all_gather | solution.py:16
  653.9 39.6 %reduce-scatter.3.cloned.1.call-done = bf16[64,2048]{1,0:T(8,128)(2,1)} async-done(((bf16[128,2048]{1,0:T(8,128)(2,1)}), bf16[64,2048]{1,0:T(8,128)(2,1)}) %reduce-scatter.3.cloned.1.call-update) | async-done | bytes 262160 | tf_op jit(solution)/shard_map/reduce_scatter | solution.py:176
  697.9 140.8 %all-gather.11.cloned.1.call-done = bf16[2048,2816]{1,0:T(8,128)(2,1)} async-done(((bf16[128,2816]{1,0:T(8,128)(2,1)}), bf16[2048,2816]{1,0:T(8,128)(2,1)}) %all-gather.11.cloned.1.call-update) | async-done | bytes 11534352 | tf_op jit(solution)/shard_map/all_gather | solution.py:157
  838.6 5.9 convolution_convert_fusion.1
  848.2 132.7 %all-gather.15.cloned.1.call-done = bf16[45056,128]{1,0:T(8,128)(2,1)} async-done(((bf16[2816,128]{1,0:T(8,128)(2,1)}), bf16[45056,128]{1,0:T(8,128)(2,1)}) %all-gather.15.cloned.1.call-update) | async-done | bytes 11534352 | tf_op jit(solution)/shard_map/all_gather | solution.py:159
  980.9 15.2 %copy.92 = bf16[2816,16,128]{0,2,1:T(8,128)(2,1)} copy(bf16[2816,16,128]{2,0,1:T(8,128)(2,1)} %bitcast.190) | data formatting | bytes 23068672 | tf_op jit(solution)/shard_map/reshape | solution.py:159
  997.5 125.7 %all-gather.13.cloned.1.call-done = bf16[2048,2816]{1,0:T(8,128)(2,1)} async-done(((bf16[128,2816]{1,0:T(8,128)(2,1)}), bf16[2048,2816]{1,0:T(8,128)(2,1)}) %all-gather.13.cloned.1.call-update) | async-done | bytes 11534352 | tf_op jit(solution)/shard_map/all_gather | solution.py:158
  1123.1 14.8 %convolution_convert_fusion.2 = bf16[128,2048]{1,0:T(8,128)(2,1)} fusion(bf16[2816,2048]{0,1:T(8,128)(2,1)} %bitcast.191, bf16[128,2048]{1,0:T(8,128)(2,1)S(1)} %all_gather.25, bf16[2048,2816]{1,0:T(8,128)(2,1)} %all-gather.13.cloned.1.call-done, f32[130,2816]{1,0:T(8,128)} %maximum_convert_fusion, f32[2816]{0:T(1024)S(1)} %get-tuple-element.204, ...), kind=kOutput, calls=%fused_computation.27 | convolution fusion | flops 2957737984 | bytes 28476416 | tf_op jit(solution)/shard_map/dot_general | solution.py:205
  1137.9 6.3 reduce-scatter.5.cloned.1.call-done
  (429 shorter events, 477.2 us)
Async XLA Ops:
  6.5 643.3 %copy-start = (bf16[512,2048]{1,0:T(8,128)(2,1)S(1)}, bf16[512,2048]{1,0:T(8,128)(2,1)}, u32[]{:S(2)}) copy-start(bf16[512,2048]{1,0:T(8,128)(2,1)} %param.27) | copy-start | bytes 6291460
  6.5 587.1 %all-gather.9.cloned.1.call-start = ((), (), s32[]{:S(2)}) async-start(), calls=%async_computation.3 | async-start | bytes 2228224 | tf_op jit(solution)/shard_map/all_gather | solution.py:16
  7.9 13.7 %copy-start.22 = (f32[64,64]{1,0:T(8,128)}, f32[64,64]{1,0:T(8,128)S(1)}, u32[]{:S(2)}) copy-start(f32[64,64]{1,0:T(8,128)S(1)} %fusion.61) | copy-start | bytes 49156
  48.5 10.0 copy-start.4
  74.7 10.0 copy-start.4
  100.9 10.0 copy-start.4
  127.1 10.0 copy-start.4
  153.3 10.0 copy-start.4
  450.4 10.9 slice-start
  478.2 16.5 %copy-start.18 = (f32[1,8,64,64]{3,2,1,0:T(8,128)S(1)}, f32[1,8,64,64]{3,2,1,0:T(8,128)}, u32[]{:S(2)}) copy-start(f32[1,8,64,64]{3,2,1,0:T(8,128)} %slice.129) | copy-start | bytes 393220
  515.3 125.3 %all-gather.7.cloned.1.call-start = ((), (), s32[]{:S(2)}) async-start(), calls=%async_computation.2 | async-start | bytes 2228224 | tf_op jit(solution)/shard_map/all_gather | solution.py:16
  545.3 148.1 %reduce-scatter.3.cloned.1.call-start = ((), (), s32[]{:S(2)}) async-start(), calls=%async_computation.4 | async-start | bytes 786432 | tf_op jit(solution)/shard_map/reduce_scatter | solution.py:176
  576.0 11.1 copy-start.27
  576.0 11.2 copy-start.17
  652.1 41.4 %copy-start.12 = (bf16[64,2048]{1,0:T(8,128)(2,1)S(1)}, bf16[64,2048]{1,0:T(8,128)(2,1)}, u32[]{:S(2)}) copy-start(bf16[64,2048]{1,0:T(8,128)(2,1)} %param.28) | copy-start | bytes 786436
  652.1 42.6 %copy-start.25 = (f32[2048]{0:T(1024)S(1)}, f32[2048]{0:T(1024)}, u32[]{:S(2)}) copy-start(f32[2048]{0:T(1024)} %param.29) | copy-start | bytes 24580
  652.1 186.6 %all-gather.11.cloned.1.call-start = ((), (), s32[]{:S(2)}) async-start(), calls=%async_computation.5 | async-start | bytes 12255232 | tf_op jit(solution)/shard_map/all_gather | solution.py:157
  652.7 328.2 %all-gather.15.cloned.1.call-start = ((), (), s32[]{:S(2)}) async-start(), calls=%async_computation.8 | async-start | bytes 12255232 | tf_op jit(solution)/shard_map/all_gather | solution.py:159
  653.2 469.9 %all-gather.13.cloned.1.call-start = ((), (), s32[]{:S(2)}) async-start(), calls=%async_computation.6 | async-start | bytes 12255232 | tf_op jit(solution)/shard_map/all_gather | solution.py:158
  653.8 490.4 %reduce-scatter.5.cloned.1.call-start = ((), (), s32[]{:S(2)}) async-start(), calls=%async_computation.7 | async-start | bytes 786432 | tf_op jit(solution)/shard_map/reduce_scatter | solution.py:204
  697.9 150.2 %copy-start.24 = (f32[3,2816]{1,0:T(4,128)S(1)}, f32[3,2816]{1,0:T(4,128)}, u32[]{:S(2)}) copy-start(f32[3,2816]{1,0:T(4,128)} %param.32) | copy-start | bytes 101380
  844.6 151.5 %collective-permute-start = (bf16[2,2816]{1,0:T(2,128)(2,1)S(1)}, bf16[2,2816]{1,0:T(2,128)(2,1)S(1)}, u32[]{:S(2)}, u32[]{:S(2)}) collective-permute-start(bf16[2,2816]{1,0:T(2,128)(2,1)S(1)} %slice.166), channel_id=1, source_target_pairs={{0,2},{2,4},{4,6},{6,8},{8,10},{10,12},{12,14},{14,16},{16,18},{18... | collective-permute-start | bytes 33800 | tf_op jit(solution)/shard_map/ppermute | solution.py:36
  1123.1 21.1 %copy-start.13 = (bf16[64,2048]{1,0:T(8,128)(2,1)S(1)}, bf16[64,2048]{1,0:T(8,128)(2,1)}, u32[]{:S(2)}) copy-start(bf16[64,2048]{1,0:T(8,128)(2,1)} %param.28) | copy-start | bytes 786436
  1123.1 21.1 %copy-start.14 = (bf16[64,2048]{1,0:T(8,128)(2,1)S(1)}, bf16[64,2048]{1,0:T(8,128)(2,1)}, u32[]{:S(2)}) copy-start(bf16[64,2048]{1,0:T(8,128)(2,1)} %reduce-scatter.3.cloned.1.call-done) | copy-start | bytes 786436
  (73 other events, 331.5 us)
Sparse Core Ops, SparseCore 0:
  515.4 63.0 all-gather.8
  581.3 59.1 all-gather.6
  652.2 41.2 reduce-scatter.2
  696.1 142.5 all-gather.10
  841.2 139.5 all-gather.14
  983.5 139.5 all-gather.12
  1138.0 6.1 reduce-scatter.4
